TPU v7x, 32 devices: a whole 2x2x4 slice. The times are simulated.
32 devices in a mesh: ep: 8 (over z, x), tp: 4 (over y, core).
Axes of the slice: x: 2, y: 2, z: 4, core: 2. Of those that a mesh axis runs over, the one named last changes fastest.
Arguments:
- out_gate: bfloat16 [4096, 2048], P(('ep', 'tp')), may hold values from -6 to 6
- in_gate: bfloat16 [4096, 2048], P(('ep', 'tp')), may hold values from -6 to 6
- conv_input: bfloat16 [4096, 2048], P(('ep', 'tp')), may hold values from -6 to 6
- conv_taps: bfloat16 [3, 2048], replicated, may hold values from -3 to 3
- mixer_weight: bfloat16 [2048, 2048], P(None, 'tp'), may hold values from -0.125 to 0.125
- expert_input: bfloat16 [4096, 2048], P(('ep', 'tp')), may hold values from -6 to 6
- norm_gain: float32 [2048], replicated, may hold values from 0.1 to 1.9
- expert_gate: bfloat16 [8, 2048, 1024], P('ep', None, 'tp'), may hold values from -0.125 to 0.125
- expert_up: bfloat16 [8, 2048, 1024], P('ep', None, 'tp'), may hold values from -0.125 to 0.125
- expert_down: bfloat16 [8, 1024, 2048], P('ep', 'tp'), may hold values from -0.1875 to 0.1875
- expert_ids: int32 [4096, 2], P(('ep', 'tp')), may hold values from 0 to 7, all different within a row; in each aligned block of 128 rows (0 to 127, 128 to 255, ...) at most 64 rows name the same one
- route_weight: float32 [4096, 2], P(('ep', 'tp')), may hold values from 0.1 to 1
Outputs:
- mixer_out: bfloat16 [4096, 2048], P('ep', 'tp')
- experts_out: bfloat16 [4096, 2048], P(('ep', 'tp'))
Inputs may be any that keep to these rules, and one draw needn't show every extreme that they name: `expert_ids`: each row names 2 different experts. Within the 128 rows of one device no expert is named by more than 64 rows, and in some devices' rows some expert is named by exactly 64.
All inputs are finite; a program needn't handle non-finite values.
Results may differ from a plain program's by a relative error of at most 0.011.
Values may be sent and summed in bfloat16 or wider, within the bound.
A program may use at most 128 MiB of HBM per device.

v0:
```python
import functools

import jax
import jax.numpy as jnp
from jax import lax
from jax.experimental import pallas as pl
from jax.experimental.pallas import tpu as pltpu
from jax.sharding import PartitionSpec as P

CONV = 3
SEQS = 1


norm_eps = 1e-06


def from_behind(value, axis, steps):
    count = lax.axis_size(axis)
    first, last = (max(0, -steps), min(count, count - steps))
    return lax.ppermute(value, axis, [(source, source + steps) for source in range(first, last)])


def device_slots(route_ids, expert_count):
    flat_ids = route_ids.reshape(-1)
    member = (flat_ids[:, None] == jnp.arange(expert_count, dtype=jnp.int32)[None, :]).astype(
        jnp.int32
    )
    before = jnp.cumsum(member, axis=0) - member
    return jnp.sum(before * member, axis=1).reshape(route_ids.shape)


def fill_slots(row_data, route_ids, expert_count, slot_cap):
    top_count = route_ids.shape[1]
    position = (route_ids * slot_cap + device_slots(route_ids, expert_count)).reshape(-1)
    zeroed = jnp.zeros((expert_count * slot_cap, row_data.shape[1]), row_data.dtype)
    return zeroed.at[position].set(jnp.repeat(row_data, top_count, axis=0))


def expert_hidden(slot_rows, w_gate, w_up):
    gate_proj = jnp.dot(slot_rows, w_gate, preferred_element_type=jnp.float32)
    up_proj = jnp.dot(slot_rows, w_up, preferred_element_type=jnp.float32)
    return (jax.nn.silu(gate_proj) * up_proj).astype(jnp.bfloat16)


def local(
    out_gate,
    in_gate,
    conv_input,
    conv_taps,
    mixer_weight,
    expert_input,
    norm_gain,
    expert_gate,
    expert_up,
    expert_down,
    expert_ids,
    route_weight,
):
    row_count = in_gate.shape[0]
    tap_span = CONV - 1
    group_size = lax.axis_size("tp")
    product = in_gate.astype(jnp.float32) * conv_input.astype(jnp.float32)
    edge_product = from_behind(product[row_count - tap_span :], ("ep", "tp"), 1)
    seq_length = row_count * lax.axis_size("ep") * group_size // SEQS
    linear_index = lax.axis_index("ep") * group_size + lax.axis_index("tp")
    carry_over = jnp.where(linear_index * row_count % seq_length == 0, 0.0, 1.0).astype(jnp.float32)
    earlier = edge_product * carry_over
    padded = jnp.concatenate([earlier, product], axis=0)
    tap_values = conv_taps.astype(jnp.float32)
    smoothed = sum(
        (
            padded[tap_index : tap_index + row_count] * tap_values[tap_index]
            for tap_index in range(CONV)
        )
    )
    gated = (out_gate.astype(jnp.float32) * smoothed).astype(jnp.bfloat16)
    token_count = expert_input.shape[0]
    model_width = expert_input.shape[1]
    expert_count = lax.axis_size("ep")
    slot_cap = 4 * token_count // expert_count
    wide_input = expert_input.astype(jnp.float32)
    inv_norm = lax.rsqrt(jnp.mean(wide_input * wide_input, axis=1, keepdims=True) + norm_eps)
    normed = (wide_input * inv_norm * norm_gain).astype(jnp.bfloat16)
    w_gate = expert_gate[0]
    hidden_width = w_gate.shape[1]
    position = (expert_ids * slot_cap + device_slots(expert_ids, expert_count)).reshape(-1)
    whole_gate, whole_up, whole_down = (
        lax.all_gather(expert_gate, "tp", axis=2, tiled=True),
        lax.all_gather(expert_up, "tp", axis=2, tiled=True),
        lax.all_gather(expert_down, "tp", axis=1, tiled=True),
    )
    mixer_out = jnp.dot(
        lax.all_gather(gated, "tp", axis=0, tiled=True),
        mixer_weight,
        preferred_element_type=jnp.float32,
    ).astype(jnp.bfloat16)
    outgoing = fill_slots(normed, expert_ids, expert_count, slot_cap).reshape(
        expert_count, slot_cap, model_width
    )
    arrived = lax.all_to_all(outgoing, "ep", split_axis=0, concat_axis=0, tiled=True)
    hidden = expert_hidden(arrived.reshape(-1, model_width), whole_gate[0], whole_up[0])
    running = jnp.zeros((hidden.shape[0], model_width), jnp.float32)
    for quarter in range(group_size):
        partial_sum = jnp.dot(
            hidden[:, quarter * hidden_width : (quarter + 1) * hidden_width],
            whole_down[0, quarter * hidden_width : (quarter + 1) * hidden_width],
            preferred_element_type=jnp.float32,
        )
        running = running + lax.optimization_barrier(partial_sum.astype(jnp.bfloat16)).astype(
            jnp.float32
        )
    summed = running.astype(jnp.bfloat16)
    returned = lax.all_to_all(
        summed.reshape(expert_count, slot_cap, model_width),
        "ep",
        split_axis=0,
        concat_axis=0,
        tiled=True,
    )
    picked = returned.reshape(expert_count * slot_cap, model_width)[position]
    top_count = expert_ids.shape[1]
    picked = picked.reshape(token_count, top_count, model_width).astype(jnp.float32)
    route_share = route_weight / jnp.sum(route_weight, axis=1, keepdims=True)
    experts_out = jnp.sum(picked * route_share[:, :, None], axis=1).astype(jnp.bfloat16)
    return (mixer_out, experts_out)


MESH = pl.DeviceIdType.MESH
PIECES = 4


def fused_kernel(
    ep_size,
    tp_size,
    cap,
    x_hbm,
    gain_hbm,
    taps_hbm,
    ids_hbm,
    weight_hbm,
    og_hbm,
    ig_hbm,
    ci_hbm,
    mw_hbm,
    wg_hbm,
    wu_hbm,
    wd_hbm,
    mix_ref,
    out_ref,
    x_ref,
    gain_ref,
    taps_ref,
    ids_ref,
    weight_ref,
    og,
    ig,
    ci,
    mw,
    gates,
    ups,
    downs,
    xs,
    xr,
    hid,
    ys,
    yr,
    prod,
    gat,
    place,
    normed,
    summed,
    sums,
    info,
    their_info,
    picks,
    their_place,
    their_rows,
    local_sem,
    own_sem,
    y_send,
    y_recv,
    c_send,
    c_recv,
    f_send,
    f_recv,
    x_send,
    x_recv,
    r_send,
    r_recv,
    e_send,
    e_recv,
    g_send,
    g_recv,
    p_send,
    p_recv,
    m_send,
    m_recv,
    n_send,
    n_recv,
):
    f32, bf16 = jnp.float32, jnp.bfloat16
    ep, tp = lax.axis_index("ep"), lax.axis_index("tp")
    rows, width = x_ref.shape
    x_copies, og_copies = (2, 3, 4, 7), (5, 6)
    piece = width // PIECES
    tp_c = tp + 1 - 2 * lax.rem(tp, 2)
    tp_y = lax.rem(tp + 2, tp_size)
    line = ep * tp_size + tp
    count = ep_size * tp_size
    after, before = lax.rem(line + 1, count), lax.rem(line + count - 1, count)
    after_id = (after // tp_size, lax.rem(after, tp_size))
    before_id = (before // tp_size, lax.rem(before, tp_size))
    core_id, y_id = (ep, tp_c), (ep, tp_y)

    bits = [1 << b for b in range(ep_size.bit_length() - 1)]
    half = ep_size // 2

    def peer(k):
        return sum(lax.rem(ep // b + k // b, 2) * b for b in bits)

    barrier = pltpu.get_barrier_semaphore()
    partners = [(peer(k), tp) for k in range(1, ep_size)] + [core_id, y_id, after_id, before_id]
    for partner in partners:
        pl.semaphore_signal(barrier, inc=1, device_id=partner, device_id_type=MESH)

    stage = [
        pltpu.make_async_copy(s, d, local_sem.at[i])
        for i, (s, d) in enumerate(
            (
                (ig_hbm, ig),
                (ci_hbm, ci),
                (x_hbm, x_ref),
                (ids_hbm, ids_ref),
                (gain_hbm, gain_ref),
                (og_hbm, og),
                (taps_hbm, taps_ref),
                (weight_hbm, weight_ref),
                (mw_hbm, mw),
            )
        )
    ]
    for copy in stage:
        copy.start()

    def parts(owner):
        cut = [(wg_hbm, gates.at[owner]), (wu_hbm, ups.at[owner])]
        for j in range(PIECES):
            cut.append((wd_hbm.at[:, pl.ds(j * piece, piece)], downs.at[j, owner]))
        return cut

    def remote(s, d, ss, rs, who):
        return pltpu.make_async_remote_copy(
            src_ref=s, dst_ref=d, send_sem=ss, recv_sem=rs, device_id=who, device_id_type=MESH
        )

    own = [pltpu.make_async_copy(s, d, own_sem.at[i]) for i, (s, d) in enumerate(parts(tp))]
    for copy in own:
        copy.start()
    head = 8
    strip = 256
    stage[0].wait()
    stage[1].wait()

    def multiply(i, carry):
        c = pl.ds(pl.multiple_of(i * strip, strip), strip)
        prod[head : head + rows, c] = ig[:, c].astype(f32) * ci[:, c].astype(f32)
        return carry

    lax.fori_loop(0, width // strip, multiply, 0)
    edge = remote(prod.at[rows : rows + head], prod.at[0:head], e_send, e_recv, after_id)
    pl.semaphore_wait(barrier, len(partners))
    edge.start()
    to_y = [remote(s, d, y_send.at[i], y_recv.at[i], y_id) for i, (s, d) in enumerate(parts(tp))]
    to_c = [remote(s, d, c_send.at[i], c_recv.at[i], core_id) for i, (s, d) in enumerate(parts(tp))]
    for copy in to_y + to_c:
        copy.start()

    for i in x_copies:
        stage[i].wait()
    ids_row = ids_ref[...]
    info[...] = jnp.concatenate(
        [ids_row.astype(f32), weight_ref[...], jnp.zeros((4, rows), f32)], axis=0
    )
    mirror = peer(half)
    tell = remote(info, their_info, m_send, m_recv, (mirror, tp))
    tell.start()
    lanes = place.shape[1]
    near = ep // half
    far = 1 - near
    turn = (far - near) * half
    ti = lax.broadcasted_iota(jnp.int32, (rows, rows), 0)
    tj = lax.broadcasted_iota(jnp.int32, (rows, rows), 1)
    upper = jnp.where(ti < tj, 1.0, 0.0).astype(bf16)
    expert_row = lax.broadcasted_iota(jnp.int32, place.shape, 0).astype(f32)

    def rank_rows(source, target):
        member = (source[0:1, :] == expert_row) | (source[1:2, :] == expert_row)
        member = jnp.where(member, 1.0, 0.0)
        rank = jnp.dot(member.astype(bf16), upper, preferred_element_type=f32)
        target[...] = jnp.where(member > 0.5, rank, -1.0)

    rank_rows(info, place)
    wide = x_ref[...].astype(f32)
    inv = lax.rsqrt(jnp.mean(wide * wide, axis=1, keepdims=True) + norm_eps)
    normed[...] = (wide * inv * gain_ref[...]).astype(bf16)
    slot = lax.broadcasted_iota(jnp.int32, (cap, rows), 0).astype(f32)
    across_rows = remote(normed, their_rows, n_send, n_recv, (mirror, tp))
    across_rows.start()

    def chosen(e, places, source):
        pick = jnp.where(places[pl.ds(e, 1), :] == slot, 1.0, 0.0).astype(bf16)
        return jnp.dot(pick, source[...], preferred_element_type=f32).astype(bf16)

    def send_rows(places, source, shift):
        def body(i, carry):
            e = peer(half - 1 - i)
            xs[e + shift] = chosen(e, places, source)
            remote(
                xs.at[e + shift],
                xr.at[ep + shift],
                x_send.at[e + shift],
                x_recv.at[ep + shift],
                (e, tp),
            ).start()
            return carry

        lax.fori_loop(0, half - 1, body, 0)
        xr[ep + shift] = chosen(ep, places, source)

    send_rows(place, normed, 0)

    for i in og_copies:
        stage[i].wait()
    edge.wait()

    @pl.when(line * rows % (rows * count // SEQS) == 0)
    def _():
        prod[0:head, :] = jnp.zeros((head, width), f32)

    def smooth(i, carry):
        c = pl.ds(pl.multiple_of(i * strip, strip), strip)
        taps = taps_ref[:, c].astype(f32)
        total = prod[head : head + rows, c] * taps[CONV - 1 : CONV]
        for j in range(CONV - 1):
            lo = head - (CONV - 1) + j
            total = total + prod[lo : lo + rows, c] * taps[j : j + 1]
        gat[tp, :, c] = (og[:, c].astype(f32) * total).astype(bf16)
        return carry

    lax.fori_loop(0, width // strip, smooth, 0)
    g_y = remote(gat.at[tp], gat.at[tp], g_send.at[0], g_recv.at[0], y_id)
    g_c = remote(gat.at[tp], gat.at[tp], g_send.at[1], g_recv.at[1], core_id)
    g_y.start()
    g_c.start()

    def mix(t):
        mix_ref[pl.ds(pl.multiple_of(t * rows, rows), rows), :] = jnp.dot(
            gat[t], mw[...], preferred_element_type=f32
        ).astype(bf16)

    stage[8].wait()
    g_c.wait_recv()

    def mix_two(i, carry):
        mix(2 * (tp // 2) + i)
        return carry

    lax.fori_loop(0, 2, mix_two, 0)

    lane = tj.astype(f32)
    lower = jnp.where(tj < ti, 1.0, 0.0).astype(bf16)
    slots = lax.broadcasted_iota(jnp.int32, (rows, half * cap), 1).astype(f32)
    first = (near * half).astype(f32)

    def column(row):
        return jnp.sum(jnp.where(ti == tj, row, 0.0), axis=1, keepdims=True)

    def route(source, target):
        named = [column(source[k : k + 1, :]) for k in range(2)]
        weight = [column(source[2 + k : 3 + k, :]) for k in range(2)]
        member = jnp.where((named[0] == lane) | (named[1] == lane), 1.0, 0.0).astype(bf16)
        ranks = jnp.dot(lower, member, preferred_element_type=f32)
        for k in range(2):
            rank = jnp.sum(jnp.where(lane == named[k], ranks, 0.0), axis=1, keepdims=True)
            at = (named[k] - first) * cap + rank
            picks[target, k] = jnp.where(slots == at, 1.0, 0.0).astype(bf16)
        return [weight[k] / (weight[0] + weight[1]) for k in range(2)]

    shares = [route(info, 0)]
    tell.wait()
    shares.append(route(their_info, 1))

    def weighted(j, target):
        block = yr[j, target].reshape(half * cap, piece)
        total = shares[target][0] * jnp.dot(picks[target, 0], block, preferred_element_type=f32)
        return total + shares[target][1] * jnp.dot(
            picks[target, 1], block, preferred_element_type=f32
        )

    rank_rows(their_info, their_place)
    across_rows.wait()
    send_rows(their_place, their_rows, turn)

    dest_y = parts(tp_y)
    forward = [
        remote(d, d, f_send.at[i], f_recv.at[i], core_id) for i, (_, d) in enumerate(dest_y)
    ]

    def arrive(k, carry):
        s = peer(k)
        remote(xs.at[s], xr.at[s], x_send.at[s], x_recv.at[s], (s, tp)).wait()
        return carry

    def hidden(q, side):
        x = xr[pl.ds(side * half, half)].reshape(half * cap, width)
        g = jnp.dot(x, gates[q], preferred_element_type=f32)
        u = jnp.dot(x, ups[q], preferred_element_type=f32)
        at = pl.ds(pl.multiple_of(side * (half * cap), half * cap), half * cap)
        hid[q, at, :] = (g / (1.0 + jnp.exp(-g)) * u).astype(bf16)

    chip, chip_other = 2 * (tp // 2), 1 - 2 * lax.rem(tp, 2)
    lax.fori_loop(1, half, arrive, 0)
    for i in range(2):
        own[i].wait()
        to_c[i].wait_recv()

    def both_halves(q):
        def body(i, carry):
            hidden(q, i)
            return carry

        lax.fori_loop(0, 2, body, 0)

    def hidden_chip(i, carry):
        hidden(chip + lax.rem(i, 2), near + (i // 2) * (far - near))

        @pl.when(i == 1)
        def _():
            to_y[0].wait_recv()
            forward[0].start()
            lax.fori_loop(half + 1, ep_size, arrive, 0)

        return carry

    lax.fori_loop(0, 4, hidden_chip, 0)
    to_y[1].wait_recv()
    forward[1].start()
    both_halves(tp_y)
    for m in range(2):
        forward[m].wait_recv()
    both_halves(tp_y + chip_other)

    mine = ep - near * half

    def give_back(j, kind, s):
        return remote(
            ys.at[j, s + kind * turn],
            yr.at[j, kind, mine],
            r_send.at[j, kind, s - near * half],
            r_recv.at[j, kind, mine],
            (s, tp),
        )

    def send_all(j, kind):
        def body(k, carry):
            give_back(j, kind, peer(half - 1 - k)).start()
            return carry

        lax.fori_loop(0, half - 1, body, 0)

    def wait_all(j, kind):
        def body(k, carry):
            s = peer(k)
            at = s - near * half
            remote(
                ys.at[j, s + kind * turn],
                yr.at[j, kind, at],
                r_send.at[j, kind, at],
                r_recv.at[j, kind, at],
                (s, tp),
            ).wait()
            return carry

        lax.fori_loop(1, half, body, 0)

    across_half = [
        remote(summed.at[j], sums.at[j], p_send.at[j], p_recv.at[j], (mirror, tp))
        for j in range(PIECES)
    ]

    def relay(j):
        wait_all(j, 1)
        summed[j] = weighted(j, 1).astype(bf16)
        across_half[j].start()

    for j in range(PIECES):
        m = 2 + j
        to_y[m].wait_recv()
        forward[m].start()
        own[m].wait()
        to_c[m].wait_recv()
        forward[m].wait_recv()
        total = jnp.dot(hid[0], downs[j, 0], preferred_element_type=f32)
        for q in range(1, tp_size):
            total = total + jnp.dot(hid[q], downs[j, q], preferred_element_type=f32)
        ys[j] = total.astype(bf16).reshape(ep_size, cap, piece)
        yr[j, 0, mine] = ys[j, ep]
        yr[j, 1, mine] = ys[j, mirror]
        send_all(j, 1)
        if j:
            relay(j - 1)
        send_all(j, 0)

    g_y.wait_recv()
    g_f = remote(gat.at[tp_y], gat.at[tp_y], g_send.at[2], g_recv.at[2], core_id)
    g_f.start()
    g_f.wait_recv()

    def mix_rest(i, carry):
        mix(2 * (tp_y // 2) + i)
        return carry

    lax.fori_loop(0, 2, mix_rest, 0)

    relay(PIECES - 1)
    for j in range(PIECES):
        wait_all(j, 0)
        across_half[j].wait()
        total = weighted(j, 0) + sums[j].astype(f32)
        out_ref[:, j * piece : (j + 1) * piece] = total.astype(bf16)

    for copy in to_y + to_c + forward + [g_y, g_c, g_f]:
        copy.wait_send()


def fused(
    out_gate,
    in_gate,
    conv_input,
    conv_taps,
    mixer_weight,
    expert_input,
    norm_gain,
    expert_gate,
    expert_up,
    expert_down,
    expert_ids,
    route_weight,
):
    ep_size, tp_size = lax.axis_size("ep"), lax.axis_size("tp")
    rows, width = expert_input.shape
    cap = 4 * rows // ep_size
    part = expert_gate.shape[2]
    columns = mixer_weight.shape[1]
    bf16, f32 = jnp.bfloat16, jnp.float32
    vmem, hbm = pl.BlockSpec(memory_space=pltpu.VMEM), pl.BlockSpec(memory_space=pltpu.HBM)
    dma = pltpu.SemaphoreType.DMA
    piece = width // PIECES
    blocks = 2 + PIECES
    return pl.pallas_call(
        functools.partial(fused_kernel, ep_size, tp_size, cap),
        out_shape=(
            jax.ShapeDtypeStruct((rows * tp_size, columns), bf16),
            jax.ShapeDtypeStruct((rows, width), bf16),
        ),
        in_specs=[hbm] * 12,
        out_specs=(vmem, vmem),
        scratch_shapes=[
            pltpu.VMEM((rows, width), bf16),
            pltpu.VMEM((1, width), f32),
            pltpu.VMEM(conv_taps.shape, bf16),
            pltpu.VMEM((expert_ids.shape[1], rows), jnp.int32),
            pltpu.VMEM((expert_ids.shape[1], rows), f32),
            pltpu.VMEM((rows, width), bf16),
            pltpu.VMEM((rows, width), bf16),
            pltpu.VMEM((rows, width), bf16),
            pltpu.VMEM(mixer_weight.shape, bf16),
            pltpu.VMEM((tp_size, width, part), bf16),
            pltpu.VMEM((tp_size, width, part), bf16),
            pltpu.VMEM((PIECES, tp_size, part, piece), bf16),
            pltpu.VMEM((ep_size, cap, width), bf16),
            pltpu.VMEM((ep_size, cap, width), bf16),
            pltpu.VMEM((tp_size, ep_size * cap, part), bf16),
            pltpu.VMEM((PIECES, ep_size, cap, piece), bf16),
            pltpu.VMEM((PIECES, 2, ep_size // 2, cap, piece), bf16),
            pltpu.VMEM((rows + 8, width), f32),
            pltpu.VMEM((tp_size, rows, width), bf16),
            pltpu.VMEM((max(8, ep_size), rows), f32),
            pltpu.VMEM((rows, width), bf16),
            pltpu.VMEM((PIECES, rows, piece), bf16),
            pltpu.VMEM((PIECES, rows, piece), bf16),
            pltpu.VMEM((8, rows), f32),
            pltpu.VMEM((8, rows), f32),
            pltpu.VMEM((2, 2, rows, ep_size // 2 * cap), bf16),
            pltpu.VMEM((max(8, ep_size), rows), f32),
            pltpu.VMEM((rows, width), bf16),
            dma((9,)),
            dma((blocks,)),
            dma((blocks,)),
            dma((blocks,)),
            dma((blocks,)),
            dma((blocks,)),
            dma((blocks,)),
            dma((blocks,)),
            dma((ep_size,)),
            dma((ep_size,)),
            dma((PIECES, 2, ep_size // 2)),
            dma((PIECES, 2, ep_size // 2)),
            dma,
            dma,
            dma((3,)),
            dma((3,)),
            dma((PIECES,)),
            dma((PIECES,)),
            dma,
            dma,
            dma,
            dma,
        ],
        compiler_params=pltpu.CompilerParams(
            collective_id=0, has_side_effects=True, vmem_limit_bytes=62 * 1024 * 1024
        ),
    )(
        expert_input,
        norm_gain.reshape(1, width),
        conv_taps,
        expert_ids.T,
        route_weight.T,
        out_gate,
        in_gate,
        conv_input,
        mixer_weight,
        expert_gate[0],
        expert_up[0],
        expert_down[0],
    )


def solution(mesh):
    ep_size, tp_size = mesh.shape["ep"], mesh.shape["tp"]
    body = fused if tp_size == 4 and ep_size <= 8 else local
    return jax.shard_map(
        body,
        mesh=mesh,
        in_specs=(
            P(("ep", "tp"), None),
            P(("ep", "tp"), None),
            P(("ep", "tp"), None),
            P(),
            P(None, "tp"),
            P(("ep", "tp"), None),
            P(),
            P("ep", None, "tp"),
            P("ep", None, "tp"),
            P("ep", "tp", None),
            P(("ep", "tp"), None),
            P(("ep", "tp"), None),
        ),
        out_specs=(P("ep", "tp"), P(("ep", "tp"), None)),
        check_vma=False,
    )
```

profile of v0, /device:TPU:0, one launch (start us, length us, event | category | flops | bytes accessed | tf_op | source)
XLA Modules:
  0.0 103.0 jit_solution(4196935773920206930)
XLA Ops:
  0.6 98.6 %shard_map.131 = (bf16[512,512]{1,0:T(8,128)(2,1)}, bf16[128,2048]{1,0:T(8,128)(2,1)}) custom-call(bf16[128,2048]{1,0:T(8,128)(2,1)} %x_hbm.1, f32[1,2048]{1,0:T(1,128)} %bitcast.9, bf16[3,2048]{1,0:T(4,128)(2,1)} %taps_hbm.1, s32[2,128]{1,0:T(2,128)} %bitcast.10, f32[2,128]{1,0:T(2,128)} %bitcast.11, bf16[128,2048]{1,0:T(8,128)(2,1)} %og_hbm.1, ...), custom_call_target="tpu_custom_call" | custom-call | tf_op jit(solution)/shard_map/pallas_call | solution.py:560
  99.3 1.9 %copy.16 = bf16[512,512]{1,0:T(8,128)(2,1)} copy(bf16[512,512]{1,0:T(8,128)(2,1)} %get-tuple-element.4) | data formatting | bytes 1048576
  101.2 1.9 %copy.17 = bf16[128,2048]{1,0:T(8,128)(2,1)} copy(bf16[128,2048]{1,0:T(8,128)(2,1)} %get-tuple-element.5) | data formatting | bytes 1048576
where the time goes:
time: 104 us; the launch traced here: 103 us
  Pallas kernels  98.6 us (95%)
  local copies, waits for them, and re-layouts  3.75 us (4%)
    pallas_call x1, Pallas kernels, fused(): pl.pallas_call(functools.partial(fused_kernel, ep_size, tp_size, cap), ou...  98.6 us
    unnamed x2, local copies, waits for them, and re-layouts  3.75 us

commit v1 on v0

--- a/solution.py
+++ b/solution.py
@@ -126,7 +126,10 @@
 
 
 MESH = pl.DeviceIdType.MESH
-PIECES = 4
+PIECES = 8
+SPLITS = 4
+EAGER = 3
+BEHIND = 2
 
 
 def fused_kernel(
@@ -162,6 +165,8 @@
     xs,
     xr,
     hid,
+    g_sum,
+    u_sum,
     ys,
     yr,
     prod,
@@ -203,6 +208,8 @@
     rows, width = x_ref.shape
     x_copies, og_copies = (2, 3, 4, 7), (5, 6)
     piece = width // PIECES
+    depth = width // SPLITS
+    part = wd_hbm.shape[0]
     tp_c = tp + 1 - 2 * lax.rem(tp, 2)
     tp_y = lax.rem(tp + 2, tp_size)
     line = ep * tp_size + tp
@@ -219,7 +226,7 @@
         return sum(lax.rem(ep // b + k // b, 2) * b for b in bits)
 
     barrier = pltpu.get_barrier_semaphore()
-    partners = [(peer(k), tp) for k in range(1, ep_size)] + [core_id, y_id, after_id, before_id]
+    partners = [(peer(k), tp) for k in range(1, half + 1)] + [core_id, y_id, after_id, before_id]
     for partner in partners:
         pl.semaphore_signal(barrier, inc=1, device_id=partner, device_id_type=MESH)
 
@@ -243,9 +250,13 @@
         copy.start()
 
     def parts(owner):
-        cut = [(wg_hbm, gates.at[owner]), (wu_hbm, ups.at[owner])]
+        cut = [(wg_hbm, gates.at[owner])]
+        for k in range(SPLITS):
+            deep = pl.ds(k * depth, depth)
+            cut.append((wu_hbm.at[deep], ups.at[owner, deep]))
+        at = pl.ds(pl.multiple_of(owner * part, part), part)
         for j in range(PIECES):
-            cut.append((wd_hbm.at[:, pl.ds(j * piece, piece)], downs.at[j, owner]))
+            cut.append((wd_hbm.at[:, pl.ds(j * piece, piece)], downs.at[j, at]))
         return cut
 
     def remote(s, d, ss, rs, who):
@@ -253,27 +264,35 @@
             src_ref=s, dst_ref=d, send_sem=ss, recv_sem=rs, device_id=who, device_id_type=MESH
         )
 
-    own = [pltpu.make_async_copy(s, d, own_sem.at[i]) for i, (s, d) in enumerate(parts(tp))]
+    def taken(ref, sem):
+        pltpu.make_async_copy(ref, ref, sem).wait()
+
+    group = [0] * (1 + SPLITS) + [1] * PIECES
+    held = (gates.at[0:2], gates.at[0])
+    own = [pltpu.make_async_copy(s, d, own_sem.at[g]) for g, (s, d) in zip(group, parts(tp))]
     for copy in own:
         copy.start()
     head = 8
     strip = 256
     stage[0].wait()
     stage[1].wait()
+    last = slice(rows - head, rows)
+    prod[rows : rows + head, :] = ig[last, :].astype(f32) * ci[last, :].astype(f32)
+    edge = remote(prod.at[rows : rows + head], prod.at[0:head], e_send, e_recv, after_id)
+    to_y = [remote(s, d, y_send, y_recv.at[i], y_id) for i, (s, d) in enumerate(parts(tp))]
+    to_c = [remote(s, d, c_send, c_recv.at[g], core_id) for g, (s, d) in zip(group, parts(tp))]
+    pl.semaphore_wait(barrier, len(partners))
+    edge.start()
+    for copy in to_y + to_c:
+        copy.start()
 
     def multiply(i, carry):
         c = pl.ds(pl.multiple_of(i * strip, strip), strip)
-        prod[head : head + rows, c] = ig[:, c].astype(f32) * ci[:, c].astype(f32)
+        first = slice(0, rows - head)
+        prod[head:rows, c] = ig[first, c].astype(f32) * ci[first, c].astype(f32)
         return carry
 
     lax.fori_loop(0, width // strip, multiply, 0)
-    edge = remote(prod.at[rows : rows + head], prod.at[0:head], e_send, e_recv, after_id)
-    pl.semaphore_wait(barrier, len(partners))
-    edge.start()
-    to_y = [remote(s, d, y_send.at[i], y_recv.at[i], y_id) for i, (s, d) in enumerate(parts(tp))]
-    to_c = [remote(s, d, c_send.at[i], c_recv.at[i], core_id) for i, (s, d) in enumerate(parts(tp))]
-    for copy in to_y + to_c:
-        copy.start()
 
     for i in x_copies:
         stage[i].wait()
@@ -311,15 +330,15 @@
         pick = jnp.where(places[pl.ds(e, 1), :] == slot, 1.0, 0.0).astype(bf16)
         return jnp.dot(pick, source[...], preferred_element_type=f32).astype(bf16)
 
-    def send_rows(places, source, shift):
+    def send_rows(places, source, shift, which):
         def body(i, carry):
             e = peer(half - 1 - i)
             xs[e + shift] = chosen(e, places, source)
             remote(
                 xs.at[e + shift],
                 xr.at[ep + shift],
-                x_send.at[e + shift],
-                x_recv.at[ep + shift],
+                x_send,
+                x_recv.at[which],
                 (e, tp),
             ).start()
             return carry
@@ -327,7 +346,7 @@
         lax.fori_loop(0, half - 1, body, 0)
         xr[ep + shift] = chosen(ep, places, source)
 
-    send_rows(place, normed, 0)
+    send_rows(place, normed, 0, 0)
 
     for i in og_copies:
         stage[i].wait()
@@ -399,37 +418,35 @@
 
     rank_rows(their_info, their_place)
     across_rows.wait()
-    send_rows(their_place, their_rows, turn)
+    send_rows(their_place, their_rows, turn, 1)
 
     dest_y = parts(tp_y)
     forward = [
-        remote(d, d, f_send.at[i], f_recv.at[i], core_id) for i, (_, d) in enumerate(dest_y)
+        remote(d, d, f_send, f_recv.at[i], core_id) for i, (_, d) in enumerate(dest_y)
     ]
 
-    def arrive(k, carry):
-        s = peer(k)
-        remote(xs.at[s], xr.at[s], x_send.at[s], x_recv.at[s], (s, tp)).wait()
-        return carry
+    def side_rows(side):
+        return pl.ds(pl.multiple_of(side * (half * cap), half * cap), half * cap)
+
+    def units(q):
+        return pl.ds(pl.multiple_of(q * part, part), part)
+
+    def gated_units(g, u):
+        return (g / (1.0 + jnp.exp(-g)) * u).astype(bf16)
+
+    def arrived(side):
+        return xr[pl.ds(side * half, half)].reshape(half * cap, width)
 
     def hidden(q, side):
-        x = xr[pl.ds(side * half, half)].reshape(half * cap, width)
+        x = arrived(side)
         g = jnp.dot(x, gates[q], preferred_element_type=f32)
         u = jnp.dot(x, ups[q], preferred_element_type=f32)
-        at = pl.ds(pl.multiple_of(side * (half * cap), half * cap), half * cap)
-        hid[q, at, :] = (g / (1.0 + jnp.exp(-g)) * u).astype(bf16)
+        hid[side_rows(side), units(q)] = gated_units(g, u)
 
     chip, chip_other = 2 * (tp // 2), 1 - 2 * lax.rem(tp, 2)
-    lax.fori_loop(1, half, arrive, 0)
-    for i in range(2):
-        own[i].wait()
-        to_c[i].wait_recv()
-
-    def both_halves(q):
-        def body(i, carry):
-            hidden(q, i)
-            return carry
-
-        lax.fori_loop(0, 2, body, 0)
+    taken(xr.at[0 : half - 1], x_recv.at[0])
+    taken(held[0], own_sem.at[0])
+    taken(held[0], c_recv.at[0])
 
     def hidden_chip(i, carry):
         hidden(chip + lax.rem(i, 2), near + (i // 2) * (far - near))
@@ -438,17 +455,51 @@
         def _():
             to_y[0].wait_recv()
             forward[0].start()
-            lax.fori_loop(half + 1, ep_size, arrive, 0)
+            taken(xr.at[0 : half - 1], x_recv.at[1])
 
         return carry
 
     lax.fori_loop(0, 4, hidden_chip, 0)
-    to_y[1].wait_recv()
-    forward[1].start()
-    both_halves(tp_y)
-    for m in range(2):
-        forward[m].wait_recv()
-    both_halves(tp_y + chip_other)
+    crossed = (tp_y, tp_y + chip_other)
+
+    def gate_part(i):
+        def body(side, carry):
+            g_sum[i, side_rows(side), :] = jnp.dot(
+                arrived(side), gates[crossed[i]], preferred_element_type=f32
+            )
+            return carry
+
+        lax.fori_loop(0, 2, body, 0)
+
+    def up_part(i, k):
+        deep = slice(k * depth, (k + 1) * depth)
+
+        def body(side, carry):
+            at = side_rows(side)
+            x = xr[pl.ds(side * half, half), :, deep].reshape(half * cap, depth)
+            u = jnp.dot(x, ups[crossed[i], deep], preferred_element_type=f32)
+            if k:
+                u = u + u_sum[i, at, :]
+            if k < SPLITS - 1:
+                u_sum[i, at, :] = u
+            else:
+                hid[at, units(crossed[i])] = gated_units(g_sum[i, at, :], u)
+            return carry
+
+        lax.fori_loop(0, 2, body, 0)
+
+    gate_part(0)
+    forward[0].wait_recv()
+    gate_part(1)
+    for k in range(SPLITS):
+        to_y[1 + k].wait_recv()
+        forward[1 + k].start()
+        if k:
+            forward[k].wait_recv()
+            up_part(1, k - 1)
+        up_part(0, k)
+    forward[SPLITS].wait_recv()
+    up_part(1, SPLITS - 1)
 
     mine = ep - near * half
 
@@ -456,8 +507,8 @@
         return remote(
             ys.at[j, s + kind * turn],
             yr.at[j, kind, mine],
-            r_send.at[j, kind, s - near * half],
-            r_recv.at[j, kind, mine],
+            r_send,
+            r_recv.at[j, kind],
             (s, tp),
         )
 
@@ -469,22 +520,10 @@
         lax.fori_loop(0, half - 1, body, 0)
 
     def wait_all(j, kind):
-        def body(k, carry):
-            s = peer(k)
-            at = s - near * half
-            remote(
-                ys.at[j, s + kind * turn],
-                yr.at[j, kind, at],
-                r_send.at[j, kind, at],
-                r_recv.at[j, kind, at],
-                (s, tp),
-            ).wait()
-            return carry
-
-        lax.fori_loop(1, half, body, 0)
+        taken(yr.at[j, kind, 0 : half - 1], r_recv.at[j, kind])
 
     across_half = [
-        remote(summed.at[j], sums.at[j], p_send.at[j], p_recv.at[j], (mirror, tp))
+        remote(summed.at[j], sums.at[j], p_send, p_recv.at[j], (mirror, tp))
         for j in range(PIECES)
     ]
 
@@ -493,44 +532,81 @@
         summed[j] = weighted(j, 1).astype(bf16)
         across_half[j].start()
 
+    def down(j, side):
+        total = jnp.dot(hid[side_rows(side), :], downs[j], preferred_element_type=f32)
+        ys[j, pl.ds(side * half, half)] = total.astype(bf16).reshape(half, cap, piece)
+
+    def finish(j):
+        wait_all(j, 0)
+        across_half[j].wait_recv()
+        total = weighted(j, 0) + sums[j].astype(f32)
+        out_ref[:, j * piece : (j + 1) * piece] = total.astype(bf16)
+
+    taken(held[1], own_sem.at[1])
+    taken(held[1], c_recv.at[1])
     for j in range(PIECES):
-        m = 2 + j
+        m = 1 + SPLITS + j
         to_y[m].wait_recv()
         forward[m].start()
-        own[m].wait()
-        to_c[m].wait_recv()
+        if j >= BEHIND:
+            relay(j - BEHIND)
         forward[m].wait_recv()
-        total = jnp.dot(hid[0], downs[j, 0], preferred_element_type=f32)
-        for q in range(1, tp_size):
-            total = total + jnp.dot(hid[q], downs[j, q], preferred_element_type=f32)
-        ys[j] = total.astype(bf16).reshape(ep_size, cap, piece)
-        yr[j, 0, mine] = ys[j, ep]
+        down(j, far)
         yr[j, 1, mine] = ys[j, mirror]
         send_all(j, 1)
-        if j:
-            relay(j - 1)
-        send_all(j, 0)
+        down(j, near)
+        yr[j, 0, mine] = ys[j, ep]
+        if j < EAGER:
+            send_all(j, 0)
+
+    late = list(range(EAGER, PIECES))
+    for j in range(PIECES - BEHIND, PIECES):
+        for i in late[:2]:
+            send_all(i, 0)
+        late = late[2:]
+        relay(j)
+    for i in late:
+        send_all(i, 0)
 
     g_y.wait_recv()
     g_f = remote(gat.at[tp_y], gat.at[tp_y], g_send.at[2], g_recv.at[2], core_id)
     g_f.start()
+    mix(tp_y)
     g_f.wait_recv()
-
-    def mix_rest(i, carry):
-        mix(2 * (tp_y // 2) + i)
-        return carry
-
-    lax.fori_loop(0, 2, mix_rest, 0)
-
-    relay(PIECES - 1)
+    mix(tp_y + chip_other)
+
     for j in range(PIECES):
-        wait_all(j, 0)
-        across_half[j].wait()
-        total = weighted(j, 0) + sums[j].astype(f32)
-        out_ref[:, j * piece : (j + 1) * piece] = total.astype(bf16)
-
-    for copy in to_y + to_c + forward + [g_y, g_c, g_f]:
+        finish(j)
+
+    for sem in (y_send, c_send, f_send):
+        taken(gates.at[0:3], sem)
+    taken(xr.at[0 : 2 * (half - 1)], x_send)
+    taken(xr.at[0 : 2 * (half - 1)], r_send)
+    taken(summed, p_send)
+    for copy in [g_y, g_c, g_f]:
         copy.wait_send()
+
+
+def place_kernel(mix_ref, out_ref, mix_hbm, out_hbm, sem):
+    copies = [
+        pltpu.make_async_copy(mix_ref, mix_hbm, sem.at[0]),
+        pltpu.make_async_copy(out_ref, out_hbm, sem.at[1]),
+    ]
+    for copy in copies:
+        copy.start()
+    for copy in copies:
+        copy.wait()
+
+
+def placed(mix, out):
+    vmem, hbm = pl.BlockSpec(memory_space=pltpu.VMEM), pl.BlockSpec(memory_space=pltpu.HBM)
+    return pl.pallas_call(
+        place_kernel,
+        out_shape=tuple(jax.ShapeDtypeStruct(a.shape, a.dtype) for a in (mix, out)),
+        in_specs=[vmem, vmem],
+        out_specs=(hbm, hbm),
+        scratch_shapes=[pltpu.SemaphoreType.DMA((2,))],
+    )(mix, out)
 
 
 def fused(
@@ -556,12 +632,12 @@
     vmem, hbm = pl.BlockSpec(memory_space=pltpu.VMEM), pl.BlockSpec(memory_space=pltpu.HBM)
     dma = pltpu.SemaphoreType.DMA
     piece = width // PIECES
-    blocks = 2 + PIECES
-    return pl.pallas_call(
+    blocks = 1 + SPLITS + PIECES
+    mix, out = pl.pallas_call(
         functools.partial(fused_kernel, ep_size, tp_size, cap),
         out_shape=(
-            jax.ShapeDtypeStruct((rows * tp_size, columns), bf16),
-            jax.ShapeDtypeStruct((rows, width), bf16),
+            pltpu.VMEM((rows * tp_size, columns), bf16),
+            pltpu.VMEM((rows, width), bf16),
         ),
         in_specs=[hbm] * 12,
         out_specs=(vmem, vmem),
@@ -577,10 +653,12 @@
             pltpu.VMEM(mixer_weight.shape, bf16),
             pltpu.VMEM((tp_size, width, part), bf16),
             pltpu.VMEM((tp_size, width, part), bf16),
-            pltpu.VMEM((PIECES, tp_size, part, piece), bf16),
+            pltpu.VMEM((PIECES, tp_size * part, piece), bf16),
             pltpu.VMEM((ep_size, cap, width), bf16),
             pltpu.VMEM((ep_size, cap, width), bf16),
-            pltpu.VMEM((tp_size, ep_size * cap, part), bf16),
+            pltpu.VMEM((ep_size * cap, tp_size * part), bf16),
+            pltpu.VMEM((2, ep_size * cap, part), f32),
+            pltpu.VMEM((2, ep_size * cap, part), f32),
             pltpu.VMEM((PIECES, ep_size, cap, piece), bf16),
             pltpu.VMEM((PIECES, 2, ep_size // 2, cap, piece), bf16),
             pltpu.VMEM((rows + 8, width), f32),
@@ -595,22 +673,22 @@
             pltpu.VMEM((max(8, ep_size), rows), f32),
             pltpu.VMEM((rows, width), bf16),
             dma((9,)),
+            dma((2,)),
+            dma,
             dma((blocks,)),
+            dma,
+            dma((2,)),
+            dma,
             dma((blocks,)),
-            dma((blocks,)),
-            dma((blocks,)),
-            dma((blocks,)),
-            dma((blocks,)),
-            dma((blocks,)),
-            dma((ep_size,)),
-            dma((ep_size,)),
-            dma((PIECES, 2, ep_size // 2)),
-            dma((PIECES, 2, ep_size // 2)),
+            dma,
+            dma((2,)),
+            dma,
+            dma((PIECES, 2)),
             dma,
             dma,
             dma((3,)),
             dma((3,)),
-            dma((PIECES,)),
+            dma,
             dma((PIECES,)),
             dma,
             dma,
@@ -634,6 +712,8 @@
         expert_up[0],
         expert_down[0],
     )
+    held = [pltpu.with_memory_space_constraint(a, pltpu.VMEM) for a in (mix, out)]
+    return placed(*held)
 
 
 def solution(mesh):

time: 104 us -> 95.8 us (0.921)
  local copies, waits for them, and re-layouts: 3.75 us -> 0 us
  Pallas kernels: 98.6 us -> 95 us
    pallas_call x1, Pallas kernels: 98.6 us -> 94 us  [fused(): pl.pallas_call(functools.partial(fused_kernel, ep_size, tp_size, cap), ou...]
    unnamed x2 -> x0, local copies, waits for them, and re-layouts: 3.75 us -> none
where the time goes in v1:
time: 95.8 us; the launch traced here: 95.7 us
  Pallas kernels  95 us (99%)
    pallas_call x1, Pallas kernels, fused(): pl.pallas_call(functools.partial(fused_kernel, ep_size, tp_size, cap), ou...  94 us

profile of v1, /device:TPU:0, one launch (start us, length us, event | category | flops | bytes accessed | tf_op | source)
XLA Modules:
  0.0 95.7 jit_solution(559089806542239777)
XLA Ops:
  0.6 94.0 %shard_map.131 = (bf16[512,512]{1,0:T(8,128)(2,1)S(1)}, bf16[128,2048]{1,0:T(8,128)(2,1)S(1)}) custom-call(bf16[128,2048]{1,0:T(8,128)(2,1)} %x_hbm.1, f32[1,2048]{1,0:T(1,128)} %bitcast.9, bf16[3,2048]{1,0:T(4,128)(2,1)} %taps_hbm.1, s32[2,128]{1,0:T(2,128)} %bitcast.10, f32[2,128]{1,0:T(2,128)} %bitcast.11, bf16[128,2048]{1,0:T(8,128)(2,1)} %og_hbm.1, ...), custom_call_target="tpu_custom_call" | custom-call | tf_op jit(solution)/shard_map/pallas_call | solution.py:636
  94.7 1.0 %shard_map.132 = (bf16[512,512]{1,0:T(8,128)(2,1)}, bf16[128,2048]{1,0:T(8,128)(2,1)}) custom-call(bf16[512,512]{1,0:T(8,128)(2,1)S(1)} %get-tuple-element.4.mix_ref, bf16[128,2048]{1,0:T(8,128)(2,1)S(1)} %get-tuple-element.5.out_ref), custom_call_target="tpu_custom_call" | custom-call | tf_op jit(solution)/shard_map/pallas_call | solution.py:603

commit v2 on v1

--- a/solution.py
+++ b/solution.py
@@ -126,9 +126,13 @@
 
 
 MESH = pl.DeviceIdType.MESH
-PIECES = 8
-SPLITS = 4
-EAGER = 3
+SHARES = (1,1,2,2,2,2,2,2,2)
+PIECES = len(SHARES)
+SPLITS = 8
+EAGER = 4
+AHEAD = 6
+FIRST = 6
+SOON = 2
 BEHIND = 2
 
 
@@ -169,6 +173,7 @@
     u_sum,
     ys,
     yr,
+    yf,
     prod,
     gat,
     place,
@@ -178,8 +183,12 @@
     info,
     their_info,
     picks,
+    far_picks,
+    half_sums,
+    share,
     their_place,
     their_rows,
+    bypass,
     local_sem,
     own_sem,
     y_send,
@@ -202,12 +211,18 @@
     m_recv,
     n_send,
     n_recv,
+    v_send,
+    v_recv,
+    i_send,
+    q_recv,
 ):
     f32, bf16 = jnp.float32, jnp.bfloat16
     ep, tp = lax.axis_index("ep"), lax.axis_index("tp")
     rows, width = x_ref.shape
     x_copies, og_copies = (2, 3, 4, 7), (5, 6)
-    piece = width // PIECES
+    unit = width // sum(SHARES)
+    spans = [(sum(SHARES[:j]) * unit, SHARES[j] * unit) for j in range(PIECES)]
+    cols = [pl.ds(*span) for span in spans]
     depth = width // SPLITS
     part = wd_hbm.shape[0]
     tp_c = tp + 1 - 2 * lax.rem(tp, 2)
@@ -225,10 +240,23 @@
     def peer(k):
         return sum(lax.rem(ep // b + k // b, 2) * b for b in bits)
 
+    pair = half // 2
+    near = ep // half
+    far = 1 - near
+    inner = lax.rem((ep // pair + 1) // 2, 2)
+    is_inner, is_outer = inner == 1, inner == 0
+    behind = (peer(half + pair), peer(half))
+    across = inner * behind[0] + (1 - inner) * behind[1]
     barrier = pltpu.get_barrier_semaphore()
     partners = [(peer(k), tp) for k in range(1, half + 1)] + [core_id, y_id, after_id, before_id]
+    partners.append((peer(pair), tp_y))
     for partner in partners:
         pl.semaphore_signal(barrier, inc=1, device_id=partner, device_id_type=MESH)
+
+    @pl.when(is_inner)
+    def _():
+        pl.semaphore_signal(barrier, inc=1, device_id=(behind[0], tp), device_id_type=MESH)
+
 
     stage = [
         pltpu.make_async_copy(s, d, local_sem.at[i])
@@ -256,7 +284,7 @@
             cut.append((wu_hbm.at[deep], ups.at[owner, deep]))
         at = pl.ds(pl.multiple_of(owner * part, part), part)
         for j in range(PIECES):
-            cut.append((wd_hbm.at[:, pl.ds(j * piece, piece)], downs.at[j, at]))
+            cut.append((wd_hbm.at[:, cols[j]], downs.at[at, cols[j]]))
         return cut
 
     def remote(s, d, ss, rs, who):
@@ -281,9 +309,13 @@
     edge = remote(prod.at[rows : rows + head], prod.at[0:head], e_send, e_recv, after_id)
     to_y = [remote(s, d, y_send, y_recv.at[i], y_id) for i, (s, d) in enumerate(parts(tp))]
     to_c = [remote(s, d, c_send, c_recv.at[g], core_id) for g, (s, d) in zip(group, parts(tp))]
-    pl.semaphore_wait(barrier, len(partners))
+    pl.semaphore_wait(barrier, len(partners) + inner)
     edge.start()
-    for copy in to_y + to_c:
+    around = remote(parts(tp)[1][0], bypass, y_send, v_recv, (peer(pair), tp_y))
+    to_y[0].start()
+    pl.when(is_inner)(to_y[1].start)
+    pl.when(is_outer)(around.start)
+    for copy in to_y[2:] + to_c:
         copy.start()
 
     def multiply(i, carry):
@@ -300,13 +332,10 @@
     info[...] = jnp.concatenate(
         [ids_row.astype(f32), weight_ref[...], jnp.zeros((4, rows), f32)], axis=0
     )
-    mirror = peer(half)
-    tell = remote(info, their_info, m_send, m_recv, (mirror, tp))
+    to_set = 1 - inner
+    tell = remote(info, their_info.at[to_set], m_send, m_recv.at[to_set], (across, tp))
     tell.start()
     lanes = place.shape[1]
-    near = ep // half
-    far = 1 - near
-    turn = (far - near) * half
     ti = lax.broadcasted_iota(jnp.int32, (rows, rows), 0)
     tj = lax.broadcasted_iota(jnp.int32, (rows, rows), 1)
     upper = jnp.where(ti < tj, 1.0, 0.0).astype(bf16)
@@ -323,34 +352,29 @@
     inv = lax.rsqrt(jnp.mean(wide * wide, axis=1, keepdims=True) + norm_eps)
     normed[...] = (wide * inv * gain_ref[...]).astype(bf16)
     slot = lax.broadcasted_iota(jnp.int32, (cap, rows), 0).astype(f32)
-    across_rows = remote(normed, their_rows, n_send, n_recv, (mirror, tp))
-    across_rows.start()
+    across_rows = remote(normed, their_rows.at[to_set], n_send, n_recv.at[to_set], (across, tp))
+    pl.when(is_inner)(across_rows.start)
 
     def chosen(e, places, source):
         pick = jnp.where(places[pl.ds(e, 1), :] == slot, 1.0, 0.0).astype(bf16)
         return jnp.dot(pick, source[...], preferred_element_type=f32).astype(bf16)
 
-    def send_rows(places, source, shift, which):
+    def send_rows(places, source, t, origin, which):
         def body(i, carry):
-            e = peer(half - 1 - i)
-            xs[e + shift] = chosen(e, places, source)
-            remote(
-                xs.at[e + shift],
-                xr.at[ep + shift],
-                x_send,
-                x_recv.at[which],
-                (e, tp),
-            ).start()
+            e = peer(2 - i + 3 * (i // 2))
+            at = (t - near) * half + e
+            xs[at] = chosen(e, places, source)
+            remote(xs.at[at], xr.at[origin], x_send, x_recv.at[which], (e, tp)).start()
             return carry
 
         lax.fori_loop(0, half - 1, body, 0)
-        xr[ep + shift] = chosen(ep, places, source)
-
-    send_rows(place, normed, 0, 0)
+        xr[origin] = chosen(ep, places, source)
+
+    send_rows(place, normed, 0, ep, 0)
 
     for i in og_copies:
         stage[i].wait()
-    edge.wait()
+    edge.wait_recv()
 
     @pl.when(line * rows % (rows * count // SEQS) == 0)
     def _():
@@ -385,40 +409,52 @@
         return carry
 
     lax.fori_loop(0, 2, mix_two, 0)
+    pl.when(is_outer)(across_rows.start)
 
     lane = tj.astype(f32)
     lower = jnp.where(tj < ti, 1.0, 0.0).astype(bf16)
-    slots = lax.broadcasted_iota(jnp.int32, (rows, half * cap), 1).astype(f32)
-    first = (near * half).astype(f32)
-
     def column(row):
         return jnp.sum(jnp.where(ti == tj, row, 0.0), axis=1, keepdims=True)
 
-    def route(source, target):
+    def route(source, first, target, portion):
         named = [column(source[k : k + 1, :]) for k in range(2)]
         weight = [column(source[2 + k : 3 + k, :]) for k in range(2)]
         member = jnp.where((named[0] == lane) | (named[1] == lane), 1.0, 0.0).astype(bf16)
         ranks = jnp.dot(lower, member, preferred_element_type=f32)
+        slots = lax.broadcasted_iota(jnp.int32, target.shape[1:], 1).astype(f32)
         for k in range(2):
             rank = jnp.sum(jnp.where(lane == named[k], ranks, 0.0), axis=1, keepdims=True)
-            at = (named[k] - first) * cap + rank
-            picks[target, k] = jnp.where(slots == at, 1.0, 0.0).astype(bf16)
-        return [weight[k] / (weight[0] + weight[1]) for k in range(2)]
-
-    shares = [route(info, 0)]
-    tell.wait()
-    shares.append(route(their_info, 1))
-
-    def weighted(j, target):
-        block = yr[j, target].reshape(half * cap, piece)
-        total = shares[target][0] * jnp.dot(picks[target, 0], block, preferred_element_type=f32)
-        return total + shares[target][1] * jnp.dot(
-            picks[target, 1], block, preferred_element_type=f32
-        )
-
-    rank_rows(their_info, their_place)
-    across_rows.wait()
-    send_rows(their_place, their_rows, turn, 1)
+            at = (named[k] - first.astype(f32)) * cap + rank
+            target[k] = jnp.where(slots == at, 1.0, 0.0).astype(bf16)
+            portion[k] = weight[k] / (weight[0] + weight[1])
+
+    route(info, near * half, picks, share.at[0])
+
+    def weighted(blocks, j, table, portion):
+        block = blocks[:, :, cols[j]].reshape(table.shape[2], spans[j][1])
+        total = portion[0] * jnp.dot(table[0], block, preferred_element_type=f32)
+        return total + portion[1] * jnp.dot(table[1], block, preferred_element_type=f32)
+
+    def learn(t):
+        taken(their_info.at[t], m_recv.at[t])
+        route(their_info.at[t], ep // pair * pair, far_picks.at[t], share.at[1 + t])
+
+    @pl.when(is_inner)
+    def _():
+        for t in range(2):
+            learn(t)
+            remote(
+                their_info.at[t], their_info.at[t], i_send, m_recv.at[t], (peer(pair), tp)
+            ).start()
+            rank_rows(their_info.at[t], their_place.at[t])
+            taken(their_rows.at[t], n_recv.at[t])
+            send_rows(their_place.at[t], their_rows.at[t], 1 + t, behind[t], 1)
+            if t == 0:
+                taken(bypass, v_recv)
+                deep = pl.ds(0, depth)
+                remote(
+                    bypass, ups.at[tp_y, deep], v_send, y_recv.at[1], (peer(pair), tp)
+                ).start()
 
     dest_y = parts(tp_y)
     forward = [
@@ -448,143 +484,205 @@
     taken(held[0], own_sem.at[0])
     taken(held[0], c_recv.at[0])
 
-    def hidden_chip(i, carry):
-        hidden(chip + lax.rem(i, 2), near + (i // 2) * (far - near))
-
-        @pl.when(i == 1)
-        def _():
-            to_y[0].wait_recv()
-            forward[0].start()
-            taken(xr.at[0 : half - 1], x_recv.at[1])
-
-        return carry
-
-    lax.fori_loop(0, 4, hidden_chip, 0)
     crossed = (tp_y, tp_y + chip_other)
 
-    def gate_part(i):
+    def own_units(side):
+        def body(i, carry):
+            hidden(chip + i, side)
+            return carry
+
+        lax.fori_loop(0, 2, body, 0)
+
+    def gate_part(i, side):
+        g_sum[i, side_rows(side), :] = jnp.dot(
+            arrived(side), gates[crossed[i]], preferred_element_type=f32
+        )
+
+    def up_part(i, k, side, count=1):
+        deep = slice(k * depth, (k + count) * depth)
+        at = side_rows(side)
+        x = xr[pl.ds(side * half, half), :, deep].reshape(half * cap, count * depth)
+        u = jnp.dot(x, ups[crossed[i], deep], preferred_element_type=f32)
+        if k:
+            u = u + u_sum[i, at, :]
+        if k + count < SPLITS:
+            u_sum[i, at, :] = u
+        else:
+            hid[at, units(crossed[i])] = gated_units(g_sum[i, at, :], u)
+
+    def up_both(i, k):
         def body(side, carry):
-            g_sum[i, side_rows(side), :] = jnp.dot(
-                arrived(side), gates[crossed[i]], preferred_element_type=f32
-            )
+            up_part(i, k, side)
             return carry
 
         lax.fori_loop(0, 2, body, 0)
 
-    def up_part(i, k):
-        deep = slice(k * depth, (k + 1) * depth)
-
-        def body(side, carry):
-            at = side_rows(side)
-            x = xr[pl.ds(side * half, half), :, deep].reshape(half * cap, depth)
-            u = jnp.dot(x, ups[crossed[i], deep], preferred_element_type=f32)
-            if k:
-                u = u + u_sum[i, at, :]
-            if k < SPLITS - 1:
-                u_sum[i, at, :] = u
-            else:
-                hid[at, units(crossed[i])] = gated_units(g_sum[i, at, :], u)
-            return carry
-
-        lax.fori_loop(0, 2, body, 0)
-
-    gate_part(0)
+    own_units(near)
+
+    @pl.when(is_outer)
+    def _():
+        for t in range(2):
+            learn(t)
+
+    to_y[0].wait_recv()
+    forward[0].start()
+    gate_part(0, near)
     forward[0].wait_recv()
-    gate_part(1)
-    for k in range(SPLITS):
+    gate_part(1, near)
+    for k in range(AHEAD):
         to_y[1 + k].wait_recv()
         forward[1 + k].start()
-        if k:
+        up_part(0, k, near)
+        forward[1 + k].wait_recv()
+        up_part(1, k, near)
+    pl.when(is_inner)(functools.partial(taken, xr.at[0:pair], x_recv.at[1]))
+    pl.when(is_outer)(functools.partial(taken, xr.at[0:half], x_recv.at[1]))
+    own_units(far)
+    for i in range(2):
+        gate_part(i, far)
+        up_part(i, 0, far, AHEAD)
+    for k in range(AHEAD, SPLITS):
+        to_y[1 + k].wait_recv()
+        forward[1 + k].start()
+        if k > AHEAD:
             forward[k].wait_recv()
-            up_part(1, k - 1)
-        up_part(0, k)
+            up_both(1, k - 1)
+        up_both(0, k)
+    to_y[1 + SPLITS].wait_recv()
+    forward[1 + SPLITS].start()
     forward[SPLITS].wait_recv()
-    up_part(1, SPLITS - 1)
+    up_both(1, SPLITS - 1)
 
     mine = ep - near * half
 
-    def give_back(j, kind, s):
-        return remote(
-            ys.at[j, s + kind * turn],
-            yr.at[j, kind, mine],
-            r_send,
-            r_recv.at[j, kind],
-            (s, tp),
+    own_column = lax.rem(ep, pair)
+    other_column = 1 - own_column
+
+    def send_near(j):
+        for k in (pair, 1, half - 1):
+            s = peer(k)
+            remote(
+                ys.at[s, :, cols[j]], yr.at[mine, :, cols[j]], r_send, r_recv.at[j, 0], (s, tp)
+            ).start()
+
+    def far_of(t, column):
+        return ((2 - near) if t == 0 else (3 - 3 * near)) * pair + column
+
+    def send_far(j):
+        for t in range(2):
+            remote(
+                ys.at[far_of(t, other_column), :, cols[j]],
+                yf.at[t, own_column, :, cols[j]],
+                r_send,
+                r_recv.at[j, 1],
+                (peer(1), tp),
+            ).start()
+            yf[t, own_column, :, cols[j]] = ys[far_of(t, own_column), :, cols[j]]
+
+    def collect(j, t):
+        return weighted(yf.at[t], j, far_picks.at[t], share.at[1 + t])
+
+    def pass_on(j):
+        @pl.when(is_outer)
+        def _():
+            taken(yf.at[:, 0, :, cols[j]], r_recv.at[j, 1])
+            for t in range(2):
+                summed[t, :, cols[j]] = collect(j, t).astype(bf16)
+            remote(
+                summed.at[:, :, cols[j]],
+                half_sums.at[:, :, cols[j]],
+                p_send,
+                q_recv.at[j],
+                (peer(pair), tp),
+            ).start()
+
+    def relay(j):
+        @pl.when(is_inner)
+        def _():
+            taken(yf.at[:, 0, :, cols[j]], r_recv.at[j, 1])
+            taken(half_sums.at[:, :, cols[j]], q_recv.at[j])
+            for t in range(2):
+                total = collect(j, t) + half_sums[t, :, cols[j]].astype(f32)
+                summed[t, :, cols[j]] = total.astype(bf16)
+                remote(
+                    summed.at[t, :, cols[j]],
+                    sums.at[:, cols[j]],
+                    p_send,
+                    p_recv.at[j],
+                    (behind[t], tp),
+                ).start()
+
+    def down(j, side):
+        total = jnp.dot(hid[side_rows(side), :], downs[:, cols[j]], preferred_element_type=f32)
+        ys[pl.ds(side * half, half), :, cols[j]] = total.astype(bf16).reshape(
+            half, cap, spans[j][1]
         )
 
-    def send_all(j, kind):
-        def body(k, carry):
-            give_back(j, kind, peer(half - 1 - k)).start()
-            return carry
-
-        lax.fori_loop(0, half - 1, body, 0)
-
-    def wait_all(j, kind):
-        taken(yr.at[j, kind, 0 : half - 1], r_recv.at[j, kind])
-
-    across_half = [
-        remote(summed.at[j], sums.at[j], p_send, p_recv.at[j], (mirror, tp))
-        for j in range(PIECES)
-    ]
-
-    def relay(j):
-        wait_all(j, 1)
-        summed[j] = weighted(j, 1).astype(bf16)
-        across_half[j].start()
-
-    def down(j, side):
-        total = jnp.dot(hid[side_rows(side), :], downs[j], preferred_element_type=f32)
-        ys[j, pl.ds(side * half, half)] = total.astype(bf16).reshape(half, cap, piece)
-
     def finish(j):
-        wait_all(j, 0)
-        across_half[j].wait_recv()
-        total = weighted(j, 0) + sums[j].astype(f32)
-        out_ref[:, j * piece : (j + 1) * piece] = total.astype(bf16)
+        taken(yr.at[0 : half - 1, :, cols[j]], r_recv.at[j, 0])
+        taken(sums.at[:, cols[j]], p_recv.at[j])
+        total = weighted(yr, j, picks, share.at[0]) + sums[:, cols[j]].astype(f32)
+        out_ref[:, cols[j]] = total.astype(bf16)
 
     taken(held[1], own_sem.at[1])
     taken(held[1], c_recv.at[1])
     for j in range(PIECES):
         m = 1 + SPLITS + j
-        to_y[m].wait_recv()
-        forward[m].start()
+        if j:
+            to_y[m].wait_recv()
+            forward[m].start()
+        if j >= SOON:
+            pass_on(j - SOON)
         if j >= BEHIND:
             relay(j - BEHIND)
         forward[m].wait_recv()
         down(j, far)
-        yr[j, 1, mine] = ys[j, mirror]
-        send_all(j, 1)
+        send_far(j)
         down(j, near)
-        yr[j, 0, mine] = ys[j, ep]
+        yr[mine, :, cols[j]] = ys[ep, :, cols[j]]
         if j < EAGER:
-            send_all(j, 0)
-
-    late = list(range(EAGER, PIECES))
+            send_near(j)
+        else:
+            pl.when(is_inner)(functools.partial(send_near, j))
+
+    for j in range(PIECES - SOON, PIECES):
+        pass_on(j)
+
+    @pl.when(is_outer)
+    def _():
+        for j in range(EAGER, PIECES):
+            send_near(j)
+
     for j in range(PIECES - BEHIND, PIECES):
-        for i in late[:2]:
-            send_all(i, 0)
-        late = late[2:]
         relay(j)
-    for i in late:
-        send_all(i, 0)
+
+    for j in range(FIRST):
+        finish(j)
 
     g_y.wait_recv()
     g_f = remote(gat.at[tp_y], gat.at[tp_y], g_send.at[2], g_recv.at[2], core_id)
     g_f.start()
     mix(tp_y)
+    for j in range(FIRST, PIECES - 1):
+        finish(j)
     g_f.wait_recv()
     mix(tp_y + chip_other)
-
-    for j in range(PIECES):
+    for j in range(PIECES - 1, PIECES):
         finish(j)
 
     for sem in (y_send, c_send, f_send):
         taken(gates.at[0:3], sem)
-    taken(xr.at[0 : 2 * (half - 1)], x_send)
-    taken(xr.at[0 : 2 * (half - 1)], r_send)
+    taken(xr.at[0 : half - 1], x_send)
+    taken(xr.at[0 : half + 1], r_send)
     taken(summed, p_send)
-    for copy in [g_y, g_c, g_f]:
+    for copy in [g_y, g_c, g_f, tell, across_rows, edge]:
         copy.wait_send()
+
+    @pl.when(is_inner)
+    def _():
+        taken(xr.at[0 : 2 * (half - 1)], x_send)
+        taken(their_info, i_send)
+        taken(bypass, v_send)
 
 
 def place_kernel(mix_ref, out_ref, mix_hbm, out_hbm, sem):
@@ -631,7 +729,6 @@
     bf16, f32 = jnp.bfloat16, jnp.float32
     vmem, hbm = pl.BlockSpec(memory_space=pltpu.VMEM), pl.BlockSpec(memory_space=pltpu.HBM)
     dma = pltpu.SemaphoreType.DMA
-    piece = width // PIECES
     blocks = 1 + SPLITS + PIECES
     mix, out = pl.pallas_call(
         functools.partial(fused_kernel, ep_size, tp_size, cap),
@@ -653,25 +750,30 @@
             pltpu.VMEM(mixer_weight.shape, bf16),
             pltpu.VMEM((tp_size, width, part), bf16),
             pltpu.VMEM((tp_size, width, part), bf16),
-            pltpu.VMEM((PIECES, tp_size * part, piece), bf16),
-            pltpu.VMEM((ep_size, cap, width), bf16),
+            pltpu.VMEM((tp_size * part, width), bf16),
+            pltpu.VMEM((ep_size // 2 * 3, cap, width), bf16),
             pltpu.VMEM((ep_size, cap, width), bf16),
             pltpu.VMEM((ep_size * cap, tp_size * part), bf16),
             pltpu.VMEM((2, ep_size * cap, part), f32),
             pltpu.VMEM((2, ep_size * cap, part), f32),
-            pltpu.VMEM((PIECES, ep_size, cap, piece), bf16),
-            pltpu.VMEM((PIECES, 2, ep_size // 2, cap, piece), bf16),
+            pltpu.VMEM((ep_size, cap, width), bf16),
+            pltpu.VMEM((ep_size // 2, cap, width), bf16),
+            pltpu.VMEM((2, ep_size // 4, cap, width), bf16),
             pltpu.VMEM((rows + 8, width), f32),
             pltpu.VMEM((tp_size, rows, width), bf16),
             pltpu.VMEM((max(8, ep_size), rows), f32),
             pltpu.VMEM((rows, width), bf16),
-            pltpu.VMEM((PIECES, rows, piece), bf16),
-            pltpu.VMEM((PIECES, rows, piece), bf16),
+            pltpu.VMEM((2, rows, width), bf16),
+            pltpu.VMEM((rows, width), bf16),
             pltpu.VMEM((8, rows), f32),
-            pltpu.VMEM((8, rows), f32),
-            pltpu.VMEM((2, 2, rows, ep_size // 2 * cap), bf16),
-            pltpu.VMEM((max(8, ep_size), rows), f32),
-            pltpu.VMEM((rows, width), bf16),
+            pltpu.VMEM((2, 8, rows), f32),
+            pltpu.VMEM((2, rows, ep_size // 2 * cap), bf16),
+            pltpu.VMEM((2, 2, rows, ep_size // 4 * cap), bf16),
+            pltpu.VMEM((2, rows, width), bf16),
+            pltpu.VMEM((3, 2, rows, 1), f32),
+            pltpu.VMEM((2, max(8, ep_size), rows), f32),
+            pltpu.VMEM((2, rows, width), bf16),
+            pltpu.VMEM((width // SPLITS, part), bf16),
             dma((9,)),
             dma((2,)),
             dma,
@@ -691,9 +793,13 @@
             dma,
             dma((PIECES,)),
             dma,
-            dma,
-            dma,
-            dma,
+            dma((2,)),
+            dma,
+            dma((2,)),
+            dma,
+            dma,
+            dma,
+            dma((PIECES,)),
         ],
         compiler_params=pltpu.CompilerParams(
             collective_id=0, has_side_effects=True, vmem_limit_bytes=62 * 1024 * 1024
@@ -718,7 +824,7 @@
 
 def solution(mesh):
     ep_size, tp_size = mesh.shape["ep"], mesh.shape["tp"]
-    body = fused if tp_size == 4 and ep_size <= 8 else local
+    body = fused if tp_size == 4 and ep_size == 8 else local
     return jax.shard_map(
         body,
         mesh=mesh,

time: 95.8 us -> 92.6 us (0.967)
  Pallas kernels: 95 us -> 91.6 us
    pallas_call x1, Pallas kernels: 94 us -> 90.6 us  [fused(): pl.pallas_call(functools.partial(fused_kernel, ep_size, tp_size, cap), ou...]
where the time goes in v2:
time: 92.6 us; the launch traced here: 92.4 us
  Pallas kernels  91.6 us (99%)
    pallas_call x1, Pallas kernels, fused(): pl.pallas_call(functools.partial(fused_kernel, ep_size, tp_size, cap), ou...  90.6 us

profile of v2, /device:TPU:0, one launch (start us, length us, event | category | flops | bytes accessed | tf_op | source)
XLA Modules:
  0.0 92.4 jit_solution(15180792098255601846)
XLA Ops:
  0.6 90.6 %shard_map.131 = (bf16[512,512]{1,0:T(8,128)(2,1)S(1)}, bf16[128,2048]{1,0:T(8,128)(2,1)S(1)}) custom-call(bf16[128,2048]{1,0:T(8,128)(2,1)} %x_hbm.1, f32[1,2048]{1,0:T(1,128)} %bitcast.9, bf16[3,2048]{1,0:T(4,128)(2,1)} %taps_hbm.1, s32[2,128]{1,0:T(2,128)} %bitcast.10, f32[2,128]{1,0:T(2,128)} %bitcast.11, bf16[128,2048]{1,0:T(8,128)(2,1)} %og_hbm.1, ...), custom_call_target="tpu_custom_call" | custom-call | tf_op jit(solution)/shard_map/pallas_call | solution.py:733
  91.3 1.0 %shard_map.132 = (bf16[512,512]{1,0:T(8,128)(2,1)}, bf16[128,2048]{1,0:T(8,128)(2,1)}) custom-call(bf16[512,512]{1,0:T(8,128)(2,1)S(1)} %get-tuple-element.4.mix_ref, bf16[128,2048]{1,0:T(8,128)(2,1)S(1)} %get-tuple-element.5.out_ref), custom_call_target="tpu_custom_call" | custom-call | tf_op jit(solution)/shard_map/pallas_call | solution.py:701

commit v3 on v2

--- a/solution.py
+++ b/solution.py
@@ -128,9 +128,10 @@
 MESH = pl.DeviceIdType.MESH
 SHARES = (1,1,2,2,2,2,2,2,2)
 PIECES = len(SHARES)
-SPLITS = 8
+DEEPS = (1, 4, 1, 1, 1)
+SPLITS = len(DEEPS)
 EAGER = 4
-AHEAD = 6
+AHEAD = 2
 FIRST = 6
 SOON = 2
 BEHIND = 2
@@ -223,7 +224,8 @@
     unit = width // sum(SHARES)
     spans = [(sum(SHARES[:j]) * unit, SHARES[j] * unit) for j in range(PIECES)]
     cols = [pl.ds(*span) for span in spans]
-    depth = width // SPLITS
+    depth = width // sum(DEEPS)
+    edges = [sum(DEEPS[:k]) * depth for k in range(SPLITS + 1)]
     part = wd_hbm.shape[0]
     tp_c = tp + 1 - 2 * lax.rem(tp, 2)
     tp_y = lax.rem(tp + 2, tp_size)
@@ -280,7 +282,7 @@
     def parts(owner):
         cut = [(wg_hbm, gates.at[owner])]
         for k in range(SPLITS):
-            deep = pl.ds(k * depth, depth)
+            deep = pl.ds(edges[k], edges[k + 1] - edges[k])
             cut.append((wu_hbm.at[deep], ups.at[owner, deep]))
         at = pl.ds(pl.multiple_of(owner * part, part), part)
         for j in range(PIECES):
@@ -391,10 +393,15 @@
         return carry
 
     lax.fori_loop(0, width // strip, smooth, 0)
-    g_y = remote(gat.at[tp], gat.at[tp], g_send.at[0], g_recv.at[0], y_id)
+    halves = [pl.ds(h * (rows // 2), rows // 2) for h in range(2)]
+    g_y = [
+        remote(gat.at[tp, h], gat.at[tp, h], g_send.at[0], g_recv.at[2 * n], y_id)
+        for n, h in enumerate(halves)
+    ]
     g_c = remote(gat.at[tp], gat.at[tp], g_send.at[1], g_recv.at[1], core_id)
-    g_y.start()
     g_c.start()
+    for copy in g_y:
+        copy.start()
 
     def mix(t):
         mix_ref[pl.ds(pl.multiple_of(t * rows, rows), rows), :] = jnp.dot(
@@ -499,9 +506,9 @@
         )
 
     def up_part(i, k, side, count=1):
-        deep = slice(k * depth, (k + count) * depth)
+        deep = slice(edges[k], edges[k + count])
         at = side_rows(side)
-        x = xr[pl.ds(side * half, half), :, deep].reshape(half * cap, count * depth)
+        x = xr[pl.ds(side * half, half), :, deep].reshape(half * cap, edges[k + count] - edges[k])
         u = jnp.dot(x, ups[crossed[i], deep], preferred_element_type=f32)
         if k:
             u = u + u_sum[i, at, :]
@@ -659,13 +666,18 @@
     for j in range(FIRST):
         finish(j)
 
-    g_y.wait_recv()
-    g_f = remote(gat.at[tp_y], gat.at[tp_y], g_send.at[2], g_recv.at[2], core_id)
-    g_f.start()
+    g_f = [
+        remote(gat.at[tp_y, h], gat.at[tp_y, h], g_send.at[2], g_recv.at[3 + n], core_id)
+        for n, h in enumerate(halves)
+    ]
+    for n in range(2):
+        g_y[n].wait_recv()
+        g_f[n].start()
     mix(tp_y)
     for j in range(FIRST, PIECES - 1):
         finish(j)
-    g_f.wait_recv()
+    for copy in g_f:
+        copy.wait_recv()
     mix(tp_y + chip_other)
     for j in range(PIECES - 1, PIECES):
         finish(j)
@@ -675,7 +687,9 @@
     taken(xr.at[0 : half - 1], x_send)
     taken(xr.at[0 : half + 1], r_send)
     taken(summed, p_send)
-    for copy in [g_y, g_c, g_f, tell, across_rows, edge]:
+    taken(gat.at[0], g_send.at[0])
+    taken(gat.at[0], g_send.at[2])
+    for copy in [g_c, tell, across_rows, edge]:
         copy.wait_send()
 
     @pl.when(is_inner)
@@ -773,7 +787,7 @@
             pltpu.VMEM((3, 2, rows, 1), f32),
             pltpu.VMEM((2, max(8, ep_size), rows), f32),
             pltpu.VMEM((2, rows, width), bf16),
-            pltpu.VMEM((width // SPLITS, part), bf16),
+            pltpu.VMEM((width // sum(DEEPS), part), bf16),
             dma((9,)),
             dma((2,)),
             dma,
@@ -789,7 +803,7 @@
             dma,
             dma,
             dma((3,)),
-            dma((3,)),
+            dma((5,)),
             dma,
             dma((PIECES,)),
             dma,

time: 92.6 us -> 92.7 us (level)
  no operation moved by 1% of the time
where the time goes in v3:
time: 92.7 us; the launch traced here: 92.5 us
  Pallas kernels  91.7 us (99%)
    pallas_call x1, Pallas kernels, fused(): pl.pallas_call(functools.partial(fused_kernel, ep_size, tp_size, cap), ou...  90.8 us

profile of v3, /device:TPU:0, one launch (start us, length us, event | category | flops | bytes accessed | tf_op | source)
XLA Modules:
  0.0 92.5 jit_solution(12742879487013578080)
XLA Ops:
  0.6 90.8 %shard_map.131 = (bf16[512,512]{1,0:T(8,128)(2,1)S(1)}, bf16[128,2048]{1,0:T(8,128)(2,1)S(1)}) custom-call(bf16[128,2048]{1,0:T(8,128)(2,1)} %x_hbm.1, f32[1,2048]{1,0:T(1,128)} %bitcast.9, bf16[3,2048]{1,0:T(4,128)(2,1)} %taps_hbm.1, s32[2,128]{1,0:T(2,128)} %bitcast.10, f32[2,128]{1,0:T(2,128)} %bitcast.11, bf16[128,2048]{1,0:T(8,128)(2,1)} %og_hbm.1, ...), custom_call_target="tpu_custom_call" | custom-call | tf_op jit(solution)/shard_map/pallas_call | solution.py:747
  91.4 1.0 %shard_map.132 = (bf16[512,512]{1,0:T(8,128)(2,1)}, bf16[128,2048]{1,0:T(8,128)(2,1)}) custom-call(bf16[512,512]{1,0:T(8,128)(2,1)S(1)} %get-tuple-element.4.mix_ref, bf16[128,2048]{1,0:T(8,128)(2,1)S(1)} %get-tuple-element.5.out_ref), custom_call_target="tpu_custom_call" | custom-call | tf_op jit(solution)/shard_map/pallas_call | solution.py:715
